TPU v7x, 32 devices: a whole 2x2x4 slice. The times are simulated.
32 devices in a mesh: grp: 2 (over y), kv: 4 (over z), tp: 4 (over x, core).
Axes of the slice: x: 2, y: 2, z: 4, core: 2. Of those that a mesh axis runs over, the one named last changes fastest.
Arguments:
- tokens: bfloat16 [256, 4096], P('grp', 'kv'), parts along dimension 0, may hold values from -36 to 36
- span_lengths: int32 [256], P(('grp', 'kv')), parts along dimension 0, may hold values from 1 to 256, 13107 in all
- block_state: float32 [256, 64, 32, 64], P(('grp', 'kv'), 'tp'), parts along dimension 0, may hold values from -96 to 96
- key_cache: bfloat16 [256, 2048, 256], P(('grp', 'kv'), 'tp'), parts along dimension 0, may hold values from -6 to 6
- value_cache: bfloat16 [256, 4096, 256], P(('grp', 'kv'), 'tp'), parts along dimension 0, may hold values from -6 to 6
- decay_cache: float32 [256, 2048, 256], P(('grp', 'kv'), 'tp'), parts along dimension 0, may hold values from -34 to 0, as said below
- attn_gain: float32 [4096], P('kv'), may hold values from 0.1 to 1.9
- query_weight: bfloat16 [4096, 2048], P('kv', 'tp'), may hold values from -0.09375 to 0.09375
- key_weight: bfloat16 [4096, 2048], P('kv', 'tp'), may hold values from -0.09375 to 0.09375
- value_weight: bfloat16 [4096, 4096], P('kv', 'tp'), may hold values from -0.09375 to 0.09375
- gate_weight: bfloat16 [4096, 4096], P('kv', 'tp'), may hold values from -0.09375 to 0.09375
- decay_matrix: bfloat16 [4096, 2048], P('kv', 'tp'), may hold values from -0.09375 to 0.09375
- decay_offset_bias: float32 [2048], P('tp'), may hold values from -1.4 to 6
- head_gain: float32 [64], replicated, may hold values from 0.1 to 1.9
- out_weight: bfloat16 [4096, 4096], P('tp', 'kv'), may hold values from -0.09375 to 0.09375
- mixer_gain: float32 [4096], P('kv'), may hold values from 0.1 to 1.9
- up_weight: bfloat16 [4096, 16384], P('kv', 'tp'), may hold values from -0.09375 to 0.09375
- down_weight: bfloat16 [16384, 4096], P('tp', 'kv'), may hold values from -0.046875 to 0.046875
Outputs:
- layer_out: bfloat16 [256, 4096], P('grp', 'kv'), parts along dimension 0
There are 2 independent parts, one for each index of `grp`. A program takes and returns all parts, laid end to end along the dimension named above; an argument that names none is the same for every part. Nothing has to cross between parts.
Inputs may be any that keep to these rules, and one draw needn't show every extreme that they name: Cached positions at index span_lengths - 1 and beyond are unused. `decay_cache`: Non-increasing along positions.
All inputs are finite; a program needn't handle non-finite values. No bound on the sum of `span_lengths` on one device may be relied on, other than what follows from the above.
Results may differ from a plain program's by a relative error of at most 0.005.
The roundings to bfloat16 on the way count: a program that leaves them out, or rounds other values in their place, can miss the bound.
Values may be sent and summed in bfloat16 or wider, within the bound.
A program may use at most 128 MiB of HBM per device.

v0:
```python
import jax
import jax.numpy as jnp
from jax import lax
from jax.sharding import PartitionSpec as P

D = 4096
KEY_WIDTH = 32
DV = 64


NORM_EPS = 1e-06
DECAY_SOFTNESS = 16.0


def shards(
    tokens,
    span_lengths,
    block_state,
    key_cache,
    value_cache,
    decay_cache,
    attn_gain,
    query_weight,
    key_weight,
    value_weight,
    gate_weight,
    decay_matrix,
    decay_offset_bias,
    head_gain,
    out_weight,
    mixer_gain,
    up_weight,
    down_weight,
):
    seq_count = block_state.shape[0]
    head_count = block_state.shape[1]
    span_size = key_cache.shape[2]
    whole_rows = tokens.astype(jnp.float32)
    square_sum = jnp.sum(whole_rows * whole_rows, axis=1)
    scaled = (whole_rows * attn_gain).astype(jnp.bfloat16)
    query_part = jnp.dot(scaled, query_weight, preferred_element_type=jnp.float32)
    key_part = jnp.dot(scaled, key_weight, preferred_element_type=jnp.float32)
    value_part = jnp.dot(scaled, value_weight, preferred_element_type=jnp.float32)
    gate_part = jnp.dot(scaled, gate_weight, preferred_element_type=jnp.float32)
    decay_part = jnp.dot(scaled, decay_matrix, preferred_element_type=jnp.float32)
    square_total = lax.psum(square_sum, "kv")
    query_sum, key_sum, value_sum, gate_sum, decay_running_sum = (
        lax.psum_scatter(query_part, "kv", scatter_dimension=0, tiled=True),
        lax.psum_scatter(key_part, "kv", scatter_dimension=0, tiled=True),
        lax.psum_scatter(value_part, "kv", scatter_dimension=0, tiled=True),
        lax.psum_scatter(gate_part, "kv", scatter_dimension=0, tiled=True),
        lax.psum_scatter(decay_part, "kv", scatter_dimension=0, tiled=True),
    )
    own_square = lax.dynamic_slice_in_dim(square_total, lax.axis_index("kv") * seq_count, seq_count)
    scale_per_row = lax.rsqrt(own_square / D + NORM_EPS)[:, None]
    query = (query_sum * scale_per_row * KEY_WIDTH ** (-0.5)).reshape(
        seq_count, head_count, KEY_WIDTH
    )
    key_new = (key_sum * scale_per_row).reshape(seq_count, head_count, KEY_WIDTH)
    value_new = (value_sum * scale_per_row).reshape(seq_count, head_count, DV)
    gate = gate_sum * scale_per_row
    logarithm_decay = (
        jax.nn.log_sigmoid(decay_running_sum * scale_per_row + decay_offset_bias) / DECAY_SOFTNESS
    )
    token_place = lax.broadcasted_iota(jnp.int32, (1, 1, span_size), 2)
    lengths_now = span_lengths[:, None, None]
    previous = jnp.sum(jnp.where(token_place == lengths_now - 2, decay_cache, 0.0), axis=-1)
    now_decay = (previous + logarithm_decay).reshape(seq_count, head_count, KEY_WIDTH)
    decays_span = decay_cache.reshape(seq_count, head_count, KEY_WIDTH, span_size)
    in_use = (token_place < lengths_now - 1)[:, :, None, :]
    factor = jnp.where(in_use, jnp.exp(now_decay[..., None] - decays_span), 0.0)
    keys_span = key_cache.reshape(seq_count, head_count, KEY_WIDTH, span_size)
    scores = jnp.sum(query[..., None] * keys_span.astype(jnp.float32) * factor, axis=2)
    scores_low = scores.astype(jnp.bfloat16)
    values_span = value_cache.reshape(seq_count, head_count, DV, span_size)
    history = jnp.einsum(
        "nhs,nhvs->nhv", scores_low, values_span, preferred_element_type=jnp.float32
    )
    carried = jnp.einsum(
        "nhc,nhcv->nhv", query * jnp.exp(now_decay), block_state, precision=lax.Precision.HIGHEST
    )
    own_term = jnp.sum(query * key_new, axis=-1, keepdims=True) * value_new
    raw = carried + history + own_term
    normed = raw * lax.rsqrt(jnp.mean(raw * raw, axis=-1, keepdims=True) + NORM_EPS) * head_gain
    mixed = (normed.reshape(seq_count, head_count * DV) * jax.nn.silu(gate)).astype(jnp.bfloat16)
    attn_terms = jnp.dot(
        lax.all_gather(mixed, "kv", axis=0, tiled=True),
        out_weight,
        preferred_element_type=jnp.float32,
    )
    attn_out = lax.psum(attn_terms, "tp")
    resid = (whole_rows + attn_out).astype(jnp.bfloat16)
    resid_rows = resid.astype(jnp.float32)
    mixer_square = jnp.sum(resid_rows * resid_rows, axis=1)
    mixer_scaled = (resid_rows * mixer_gain).astype(jnp.bfloat16)
    up_part = jnp.dot(mixer_scaled, up_weight, preferred_element_type=jnp.float32)
    up_share, square_share = (
        lax.psum_scatter(up_part, "kv", scatter_dimension=0, tiled=True),
        lax.psum_scatter(mixer_square, "kv", scatter_dimension=0, tiled=True),
    )
    hidden_share = jnp.square(
        jax.nn.relu(up_share * lax.rsqrt(square_share / D + NORM_EPS)[:, None])
    )
    hidden_share = hidden_share.astype(jnp.bfloat16)
    down_terms = jnp.dot(
        lax.all_gather(hidden_share, "kv", axis=0, tiled=True),
        down_weight,
        preferred_element_type=jnp.float32,
    )
    mixer_out = lax.psum(down_terms, "tp")
    return (resid_rows + mixer_out).astype(jnp.bfloat16)


def solution(mesh):
    placed = (
        P("grp", "kv"),
        P(("grp", "kv")),
        P(("grp", "kv"), "tp", None, None),
        P(("grp", "kv"), "tp", None),
        P(("grp", "kv"), "tp", None),
        P(("grp", "kv"), "tp", None),
        P("kv"),
        P("kv", "tp"),
        P("kv", "tp"),
        P("kv", "tp"),
        P("kv", "tp"),
        P("kv", "tp"),
        P("tp"),
        P(),
        P("tp", "kv"),
        P("kv"),
        P("kv", "tp"),
        P("tp", "kv"),
    )
    return jax.shard_map(
        shards, mesh=mesh, in_specs=placed, out_specs=P("grp", "kv"), check_vma=False
    )
```

profile of v0, /device:TPU:1, one launch (start us, length us, event | category | flops | bytes accessed | tf_op | source)
XLA Modules:
  0.0 291.4 jit_solution(13781271329002494492)
XLA Ops:
  6.5 0.0 reduce-scatter.7.cloned.1.call-start
  6.6 2.5 fusion.21
  9.1 0.0 reduce-scatter.7.cloned.1.call-update
  9.1 0.0 reduce-scatter.11.cloned.1.call-start
  9.2 2.4 fusion.17
  11.5 0.0 reduce-scatter.11.cloned.1.call-update
  11.5 0.0 reduce-scatter.9.cloned.1.call-start
  11.6 2.3 fusion.19
  13.9 0.0 reduce-scatter.9.cloned.1.call-update
  14.0 0.0 reduce-scatter.13.cloned.1.call-start
  14.0 2.2 fusion.15
  16.2 0.0 reduce-scatter.13.cloned.1.call-update
  16.2 0.0 reduce-scatter.15.cloned.1.call-start
  16.3 2.8 fusion.13
  19.2 0.0 reduce-scatter.15.cloned.1.call-update
  19.2 0.0 all-reduce.4.cloned.1.call-start
  19.2 0.1 fusion.3
  19.4 11.1 %psum.21 = f32[128]{0:T(128)S(1)} all-reduce(f32[128]{0:T(128)S(1)} %fusion.3), channel_id=1, replica_groups=mesh['grp'=2,'kv'=4,'tp'=4] {'kv'}, use_global_device_ids=true, to_apply=%region_2.0 | all-reduce | flops 128 | bytes 1024 | tf_op jit(solution)/shard_map/psum | solution.py:46
  30.5 0.1 iota_compare_fusion
  30.6 0.1 iota_compare_fusion.1
  30.7 0.1 add_rsqrt_fusion.1
  30.7 8.0 %select_reduce_fusion = f32[32,512]{1,0:T(8,128)S(1)} fusion(f32[32,512,256]{2,1,0:T(8,128)} %param.23, pred[32,256]{1,0:T(8,128)(4,1)S(1)} %iota_compare_fusion.1), kind=kLoop, calls=%fused_computation.3 | loop fusion | flops 8372224 | bytes 16850944 | tf_op jit(solution)/shard_map/reduce_sum | solution.py:67
  38.8 0.0 reduce-scatter.7.cloned.1.call-done
  38.8 11.0 %reduce-scatter.11.cloned.1.call-done = f32[32,512]{1,0:T(8,128)} async-done(((f32[128,512]{1,0:T(8,128)}), f32[32,512]{1,0:T(8,128)}) %reduce-scatter.11.cloned.1.call-update) | async-done | bytes 65552 | tf_op jit(solution)/shard_map/reduce_scatter | solution.py:49
  49.8 20.5 %reduce-scatter.9.cloned.1.call-done = f32[32,512]{1,0:T(8,128)} async-done(((f32[128,512]{1,0:T(8,128)}), f32[32,512]{1,0:T(8,128)}) %reduce-scatter.9.cloned.1.call-update) | async-done | bytes 65552 | tf_op jit(solution)/shard_map/reduce_scatter | solution.py:52
  70.4 1.0 fusion.25
  71.4 0.1 reshape.83
  71.5 0.1 reshape.82
  71.6 0.1 reshape.86
  71.8 0.1 exponential_multiply_fusion
  71.9 9.7 %fusion.1 = bf16[32,16,256]{2,1,0:T(8,128)(2,1)S(1)} fusion(f32[32,16,32]{2,1,0:T(8,128)S(1)} %reshape.83, f32[32,16,32]{2,1,0:T(8,128)S(1)} %reshape.82, pred[32,256]{1,0:T(8,128)(4,1)S(1)} %iota_compare_fusion, bf16[32,512,256]{2,1,0:T(8,128)(2,1)} %param.21, f32[32,512,256]{2,1,0:T(8,128)} %param.23), kind=kLoop, calls=%fused_computation.2 | loop fusion | flops 25034752 | bytes 25567232 | tf_op jit(solution)/shard_map/reduce_sum | solution.py:73
  81.6 10.2 %fusion.8 = f32[32,16,1,64]{3,2,1,0:T(1,128)S(1)} fusion(bf16[32,16,64,256]{3,2,1,0:T(8,128)(2,1)} %bitcast.34, bf16[32,16,256,1]{2,1,0,3:T(8,128)(2,1)S(1)} %bitcast.32), kind=kOutput, calls=%fused_computation.16 | convolution fusion | flops 16777216 | bytes 17170432 | tf_op jit(solution)/shard_map/nhs,nhvs->nhv/dot_general | solution.py:76
  91.8 9.2 %fusion.29 = f32[32,16,1,64]{3,2,1,0:T(1,128)S(1)} fusion(f32[32,16,32,1]{2,3,1,0:T(1,128)S(1)} %bitcast.31, f32[32,16,32,64]{3,2,1,0:T(8,128)} %param.20), kind=kOutput, calls=%fused_computation.49 | convolution fusion | flops 12582912 | bytes 4390912 | tf_op jit(solution)/shard_map/nhc,nhcv->nhv/dot_general | solution.py:79
  101.1 0.0 reduce-scatter.13.cloned.1.call-done
  101.1 1.0 broadcast_multiply_fusion
  102.1 0.1 reshape.87
  102.2 0.2 multiply_reduce_fusion
  102.5 0.1 multiply_multiply_fusion
  102.6 0.1 reshape.88
  102.8 12.9 %reduce-scatter.15.cloned.1.call-done = f32[32,1024]{1,0:T(8,128)} async-done(((f32[128,1024]{1,0:T(8,128)}), f32[32,1024]{1,0:T(8,128)}) %reduce-scatter.15.cloned.1.call-update) | async-done | bytes 131088 | tf_op jit(solution)/shard_map/reduce_scatter | solution.py:51
  115.7 1.0 multiply_convert_fusion.1
  116.7 11.0 %all_gather.6 = bf16[128,1024]{1,0:T(8,128)(2,1)S(1)} all-gather(bf16[32,1024]{1,0:T(8,128)(2,1)S(1)} %multiply_convert_fusion.1), channel_id=1, replica_groups=mesh['grp'=2,'kv'=4,'tp'=4] {'kv'}, dimensions={0}, use_global_device_ids=true | all-gather | bytes 327680 | tf_op jit(solution)/shard_map/all_gather | solution.py:87
  127.8 1.3 fusion.30
  129.0 0.0 all-reduce.4.cloned.1.call-update
  129.0 0.2 reduce-scatter.17.cloned.1.call-start
  129.3 34.7 %all-reduce.4.cloned.1.call-done = f32[128,1024]{1,0:T(8,128)} async-done(((f32[128,1024]{1,0:T(8,128)}), f32[128,1024]{1,0:T(8,128)}) %all-reduce.4.cloned.1.call-update) | async-done | bytes 524304 | tf_op jit(solution)/shard_map/psum | solution.py:91
  164.0 1.2 fusion.6
  165.2 0.0 copy-start.9
  165.2 6.0 %fusion.10 = f32[128,4096]{1,0:T(8,128)} fusion(bf16[1024,4096]{1,0:T(8,128)(2,1)} %param.34, bf16[128,1024]{1,0:T(8,128)(2,1)S(1)} %get-tuple-element.6, f32[1024]{0:T(1024)S(1)} %copy-done.5), kind=kOutput, calls=%fused_computation.19 | convolution fusion | flops 1074135040 | bytes 10752000 | tf_op jit(solution)/shard_map/dot_general | solution.py:96
  171.2 0.0 reduce-scatter.17.cloned.1.call-update
  171.2 0.0 all-gather.2.cloned.1.call-start
  171.3 0.6 dynamic-slice
  172.5 10.0 %all-reduce = f32[128]{0:T(128)S(1)} all-reduce(f32[128]{0:T(128)S(1)} %get-tuple-element.5), channel_id=8, replica_groups=mesh['grp'=2,'kv'=4,'tp'=4] {'kv'}, use_global_device_ids=true, to_apply=%region_14.15.clone | all-reduce | flops 128 | bytes 1024
  182.5 0.1 fusion.27
  182.6 33.3 %reduce-scatter.17.cloned.1.call-done = f32[32,4096]{1,0:T(8,128)} async-done(((f32[128,4096]{1,0:T(8,128)}), f32[32,4096]{1,0:T(8,128)}) %reduce-scatter.17.cloned.1.call-update) | async-done | bytes 524304 | tf_op jit(solution)/shard_map/reduce_scatter | solution.py:98
  215.9 1.9 multiply_convert_fusion
  217.8 0.0 all-gather.2.cloned.1.call-update
  217.8 0.0 copy-start.1
  217.8 0.0 all-reduce.6.cloned.1.call-start
  217.9 27.2 %all-gather.2.cloned.1.call-done = bf16[128,4096]{1,0:T(8,128)(2,1)} async-done(((bf16[32,4096]{1,0:T(8,128)(2,1)}), bf16[128,4096]{1,0:T(8,128)(2,1)}) %all-gather.2.cloned.1.call-update) | async-done | bytes 1048592 | tf_op jit(solution)/shard_map/all_gather | solution.py:106
  245.1 5.8 %fusion.31 = f32[128,1024]{1,0:T(8,128)} fusion(bf16[128,4096]{1,0:T(8,128)(2,1)} %all-gather.2.cloned.1.call-done, bf16[4096,1024]{1,0:T(8,128)(2,1)} %param.35), kind=kOutput, calls=%fused_computation.51 | convolution fusion | flops 1073741824 | bytes 9961472 | tf_op jit(solution)/shard_map/dot_general | solution.py:105
  250.8 0.0 all-reduce.6.cloned.1.call-update
  250.9 32.2 %all-reduce.6.cloned.1.call-done = f32[128,1024]{1,0:T(8,128)} async-done(((f32[128,1024]{1,0:T(8,128)}), f32[128,1024]{1,0:T(8,128)}) %all-reduce.6.cloned.1.call-update) | async-done | bytes 524304 | tf_op jit(solution)/shard_map/psum | solution.py:110
  283.1 1.8 fusion.7
  (20 shorter events, 0.0 us)
Async XLA Ops:
  6.5 7.5 %copy-start = (bf16[1024,1024]{1,0:T(8,128)(2,1)S(1)}, bf16[1024,1024]{1,0:T(8,128)(2,1)}, u32[]{:S(2)}) copy-start(bf16[1024,1024]{1,0:T(8,128)(2,1)} %param.27) | copy-start | bytes 6291460
  6.5 9.8 %copy-start.2 = (bf16[128,1024]{1,0:T(8,128)(2,1)S(1)}, bf16[128,1024]{1,0:T(8,128)(2,1)}, u32[]{:S(2)}) copy-start(bf16[128,1024]{1,0:T(8,128)(2,1)} %param.18) | copy-start | bytes 786436
  6.5 9.8 %copy-start.4 = (f32[1024]{0:T(1024)S(1)}, f32[1024]{0:T(1024)}, u32[]{:S(2)}) copy-start(f32[1024]{0:T(1024)} %param.24) | copy-start | bytes 12292
  6.5 24.0 %copy-start.8 = (s32[32]{0:T(128)S(1)}, s32[32]{0:T(128)}, u32[]{:S(2)}) copy-start(s32[32]{0:T(128)} %param.19) | copy-start | bytes 388
  6.5 32.2 %reduce-scatter.7.cloned.1.call-start = ((), (), s32[]{:S(2)}) async-start(), calls=%async_computation.6 | async-start | bytes 327680 | tf_op jit(solution)/shard_map/reduce_scatter | solution.py:48
  9.1 40.7 %reduce-scatter.11.cloned.1.call-start = ((), (), s32[]{:S(2)}) async-start(), calls=%async_computation.8 | async-start | bytes 327680 | tf_op jit(solution)/shard_map/reduce_scatter | solution.py:49
  11.5 58.8 %reduce-scatter.9.cloned.1.call-start = ((), (), s32[]{:S(2)}) async-start(), calls=%async_computation.7 | async-start | bytes 327680 | tf_op jit(solution)/shard_map/reduce_scatter | solution.py:52
  14.0 87.1 %reduce-scatter.13.cloned.1.call-start = ((), (), s32[]{:S(2)}) async-start(), calls=%async_computation.9 | async-start | bytes 655360 | tf_op jit(solution)/shard_map/reduce_scatter | solution.py:50
  16.2 99.5 %reduce-scatter.15.cloned.1.call-start = ((), (), s32[]{:S(2)}) async-start(), calls=%async_computation.10 | async-start | bytes 655360 | tf_op jit(solution)/shard_map/reduce_scatter | solution.py:51
  19.2 144.8 %all-reduce.4.cloned.1.call-start = ((), (), s32[]{:S(2)}) async-start(), calls=%async_computation.11 | async-start | bytes 1048576 | tf_op jit(solution)/shard_map/psum | solution.py:91
  30.7 39.6 %copy-start.6 = (f32[512]{0:T(512)S(1)}, f32[512]{0:T(512)}, u32[]{:S(2)}) copy-start(f32[512]{0:T(512)} %param.30) | copy-start | bytes 6148
  91.8 10.7 %copy-start.7 = (f32[64]{0:T(128)S(1)}, f32[64]{0:T(128)}, u32[]{:S(2)}) copy-start(f32[64]{0:T(128)} %param.31) | copy-start | bytes 772
  91.8 35.9 %copy-start.3 = (bf16[1024,1024]{1,0:T(8,128)(2,1)S(1)}, bf16[1024,1024]{1,0:T(8,128)(2,1)}, u32[]{:S(2)}) copy-start(bf16[1024,1024]{1,0:T(8,128)(2,1)} %param.32) | copy-start | bytes 6291460
  91.8 73.3 %copy-start.5 = (f32[1024]{0:T(1024)S(1)}, f32[1024]{0:T(1024)}, u32[]{:S(2)}) copy-start(f32[1024]{0:T(1024)} %param.33) | copy-start | bytes 12292
  129.0 86.9 %reduce-scatter.17.cloned.1.call-start = ((), (), s32[]{:S(2)}) async-start(), calls=%async_computation.12 | async-start | bytes 2621440 | tf_op jit(solution)/shard_map/reduce_scatter | solution.py:98
  165.2 6.1 %copy-start.9 = (u32[32]{0:T(128)S(1)}, u32[32]{0:T(128)}, u32[]{:S(2)}) copy-start(u32[32]{0:T(128)} %constant.44) | copy-start | bytes 388
  171.2 73.8 %all-gather.2.cloned.1.call-start = ((), (), s32[]{:S(2)}) async-start(), calls=%async_computation.13 | async-start | bytes 1310720 | tf_op jit(solution)/shard_map/all_gather | solution.py:106
  217.8 67.1 %copy-start.1 = (bf16[1024,1024]{1,0:T(8,128)(2,1)S(1)}, bf16[1024,1024]{1,0:T(8,128)(2,1)}, u32[]{:S(2)}) copy-start(bf16[1024,1024]{1,0:T(8,128)(2,1)} %param.27) | copy-start | bytes 6291460
  217.8 65.3 %all-reduce.6.cloned.1.call-start = ((), (), s32[]{:S(2)}) async-start(), calls=%async_computation.14 | async-start | bytes 1048576 | tf_op jit(solution)/shard_map/psum | solution.py:110
Sparse Core Ops, SparseCore 0:
  9.6 19.6 reduce-scatter.6
  31.5 18.2 reduce-scatter.10
  52.1 18.2 reduce-scatter.8
  72.5 20.9 reduce-scatter.12
  95.6 20.0 reduce-scatter.14
  129.2 34.7 all-reduce.3
  171.3 44.5 reduce-scatter.16
  217.9 27.0 all-gather.1
  251.0 32.0 all-reduce.5
where the time goes:
time: 294 us; the launch traced here: 291 us
  waiting for transfers between devices  172 us (59%)
  matrix products  44.8 us (15%)
  blocking collectives  32.2 us (11%)
  other arithmetic  26.6 us (9%)
  between operations  14 us (5%)
    psum x1, waiting for transfers between devices, shards(): attn_out = lax.psum(attn_terms, 'tp')  34.7 us
    reduce_scatter x1, waiting for transfers between devices, shards(): lax.psum_scatter(up_part, 'kv', scatter_dimension=0, tiled=True)  33.3 us
    psum x1, waiting for transfers between devices, shards(): mixer_out = lax.psum(down_terms, 'tp')  32.2 us
    all_gather x1, waiting for transfers between devices, shards(): lax.all_gather(hidden_share, 'kv', axis=0, tiled=True)  27.2 us
    reduce_scatter x1, waiting for transfers between devices, shards(): lax.psum_scatter(decay_part, 'kv', scatter_dimension=0, tiled=True)  20.5 us
    reduce_scatter x1, waiting for transfers between devices, shards(): lax.psum_scatter(gate_part, 'kv', scatter_dimension=0, tiled=True)  12.9 us
    psum x1, blocking collectives, shards(): square_total = lax.psum(square_sum, 'kv')  11.1 us
    reduce_scatter x1, waiting for transfers between devices, shards(): lax.psum_scatter(key_part, 'kv', scatter_dimension=0, tiled=True)  11 us
  transfers between devices with their start and end apart: 9, of which 7 were waited for; matrix products, arithmetic and copies ran while one was open for 18% of the time, Pallas kernels for 0%

commit v1 on v0

--- a/solution.py
+++ b/solution.py
@@ -1,6 +1,10 @@
+import functools
+
 import jax
 import jax.numpy as jnp
 from jax import lax
+from jax.experimental import pallas as pl
+from jax.experimental.pallas import tpu as pltpu
 from jax.sharding import PartitionSpec as P
 
 D = 4096
@@ -10,6 +14,513 @@
 
 NORM_EPS = 1e-06
 DECAY_SOFTNESS = 16.0
+MESH = pl.DeviceIdType.MESH
+LANES = 128
+F32 = jnp.float32
+BF16 = jnp.bfloat16
+
+
+def greet(axes):
+    barrier = pltpu.get_barrier_semaphore()
+    count = 0
+    for axis in axes:
+        size = lax.axis_size(axis)
+        me = lax.axis_index(axis)
+        for step in range(1, size):
+            pl.semaphore_signal(
+                barrier, inc=1, device_id={axis: lax.rem(me + step, size)}, device_id_type=MESH
+            )
+        count += size - 1
+    pl.semaphore_wait(barrier, count)
+
+
+def send(axis, step, src, dst, send_sem, recv_sem):
+    size = lax.axis_size(axis)
+    peer = lax.rem(lax.axis_index(axis) + step, size)
+    copy = pltpu.make_async_remote_copy(
+        src_ref=src(peer),
+        dst_ref=dst,
+        send_sem=send_sem,
+        recv_sem=recv_sem,
+        device_id={axis: peer},
+        device_id_type=MESH,
+    )
+    copy.start()
+    return copy
+
+
+def project_kernel(
+    parts, tok_ref, gain_ref, *refs
+):
+    weights, refs = refs[:5], refs[5:]
+    sum_ref, sq_ref = refs[:2]
+    wbuf, part, outgoing, incoming, sq_out, sq_in, wsem, ssem, rsem, qssem, qrsem = refs[2:]
+    n, rows = outgoing.shape[0], outgoing.shape[1]
+    me = lax.axis_index("kv")
+    loads = []
+    for i, (which, col, place, width) in enumerate(parts):
+        load = pltpu.make_async_copy(
+            weights[which].at[:, pl.ds(col, width)], wbuf.at[:, pl.ds(place, width)], wsem.at[i]
+        )
+        load.start()
+        loads.append(load)
+    x = tok_ref[...].astype(F32)
+    scaled = (x * gain_ref[...]).astype(BF16)
+    square = jnp.sum(x * x, axis=1, keepdims=True)
+    sq_out[...] = jnp.broadcast_to(square, (x.shape[0], LANES)).reshape(sq_out.shape)
+    greet(("kv",))
+    copies = []
+    for k in range(1, n):
+        copies.append(
+            send("kv", k, lambda p: sq_out.at[p], sq_in.at[k - 1], qssem.at[k - 1], qrsem.at[k - 1])
+        )
+    for i, (which, col, place, width) in enumerate(parts):
+        loads[i].wait()
+        cols = pl.ds(place, width)
+        got = jnp.dot(scaled, wbuf[:, cols], preferred_element_type=F32).reshape(n, rows, width)
+        part[:, :, cols] = got
+        outgoing[:, :, cols] = got.astype(BF16)
+        for k in SEND_ORDER(n):
+            copies.append(
+                send(
+                    "kv",
+                    k,
+                    lambda p: outgoing.at[p, :, cols],
+                    incoming.at[k - 1, :, cols],
+                    ssem.at[k - 1, i],
+                    rsem.at[k - 1, i],
+                )
+            )
+    for copy in copies:
+        copy.wait_recv()
+    total = part[me]
+    square = sq_out[me]
+    for k in range(n - 1):
+        total = total + incoming[k].astype(F32)
+        square = square + sq_in[k]
+    sum_ref[...] = total
+    sq_ref[...] = square
+    for copy in copies:
+        copy.wait_send()
+
+
+def SEND_ORDER(n):
+    return sorted(range(1, n), key=lambda k: -min(k, n - k))
+
+
+def project(tokens, gain, weights):
+    n = lax.axis_size("kv")
+    rows = tokens.shape[0] // n
+    parts, place = [], 0
+    for which, w in enumerate(weights):
+        width = min(512, w.shape[1])
+        for col in range(0, w.shape[1], width):
+            parts.append((which, col, place, width))
+            place += width
+    vmem = pl.BlockSpec(memory_space=pltpu.VMEM)
+    return pl.pallas_call(
+        functools.partial(project_kernel, parts),
+        out_shape=(
+            jax.ShapeDtypeStruct((rows, place), F32),
+            jax.ShapeDtypeStruct((rows, LANES), F32),
+        ),
+        in_specs=[vmem, vmem] + [pl.BlockSpec(memory_space=pltpu.HBM)] * 5,
+        out_specs=(vmem, vmem),
+        scratch_shapes=[
+            pltpu.VMEM((tokens.shape[1], place), BF16),
+            pltpu.VMEM((n, rows, place), F32),
+            pltpu.VMEM((n, rows, place), BF16),
+            pltpu.VMEM((n - 1, rows, place), BF16),
+            pltpu.VMEM((n, rows, LANES), F32),
+            pltpu.VMEM((n - 1, rows, LANES), F32),
+            pltpu.SemaphoreType.DMA((len(parts),)),
+            pltpu.SemaphoreType.DMA((n - 1, len(parts))),
+            pltpu.SemaphoreType.DMA((n - 1, len(parts))),
+            pltpu.SemaphoreType.DMA((n - 1,)),
+            pltpu.SemaphoreType.DMA((n - 1,)),
+        ],
+        compiler_params=pltpu.CompilerParams(
+            collective_id=0, has_side_effects=True, vmem_limit_bytes=40 << 20
+        ),
+        name="project",
+    )(tokens, gain.reshape(1, -1), *weights)
+
+
+NT = (((1,), (1,)), ((), ()))
+
+
+def attend_kernel(
+    len_ref, last_ref, sum_ref, sq_ref, bias_ref, hg_ref, k1, k2, d1, d2, v1, v2, st,
+    out_ref, q_t, ld_t, qk_t, vn, gs, now_s, hist, raw,
+):
+    step = pl.program_id(0)
+    rows = out_ref.shape[0]
+    heads = st.shape[1]
+    keys, vals = heads * KEY_WIDTH, heads * DV
+    lane = lax.broadcasted_iota(jnp.int32, (1, LANES), 1)
+
+    @pl.when(step == 0)
+    def _():
+        scale = lax.rsqrt(sq_ref[:, :1] / D + NORM_EPS)
+        q = sum_ref[:, :keys] * scale * KEY_WIDTH ** (-0.5)
+        key_new = sum_ref[:, keys : 2 * keys] * scale
+        at = 2 * keys
+        vn[...] = sum_ref[:, at : at + vals] * scale
+        g = sum_ref[:, at + vals : at + 2 * vals] * scale
+        gs[...] = g * (1.0 / (1.0 + jnp.exp(-g))) * jnp.concatenate([hg_ref[...]] * heads, axis=1)
+        x = sum_ref[:, at + 2 * vals :] * scale + bias_ref[...]
+        ld = (jnp.minimum(x, 0.0) - jnp.log1p(jnp.exp(-jnp.abs(x)))) / DECAY_SOFTNESS
+        spare = jnp.zeros((LANES - rows, keys), F32)
+        q_t[...] = jnp.concatenate([q, spare], axis=0).T
+        ld_t[...] = jnp.concatenate([ld, spare], axis=0).T
+        pick = lax.broadcasted_iota(jnp.int32, (heads, keys), 1) // KEY_WIDTH
+        pick = (pick == lax.broadcasted_iota(jnp.int32, (heads, keys), 0)).astype(F32)
+        qk_t[...] = lax.dot_general(
+            pick,
+            jnp.concatenate([q * key_new, spare], axis=0),
+            NT,
+            precision=lax.Precision.HIGHEST,
+            preferred_element_type=F32,
+        )
+
+    length = len_ref[step]
+    two = length - 1 > LANES
+    mine = lane == step
+    own_decay = jnp.where(mine, ld_t[...], 0.0)
+
+    @pl.when(two)
+    def _():
+        prev = jnp.where(lane + LANES == length - 2, d2[0], 0.0)
+        col = jnp.sum(own_decay + prev, axis=1, keepdims=True)
+        now_s[...] = jnp.broadcast_to(col, now_s.shape)
+
+    @pl.when(jnp.logical_not(two))
+    def _():
+        prev = jnp.where(lane == length - 2, d1[0], 0.0)
+        col = jnp.sum(own_decay + prev, axis=1, keepdims=True)
+        now_s[...] = jnp.broadcast_to(col, now_s.shape)
+
+    now = now_s[...]
+    q = jnp.broadcast_to(
+        jnp.sum(jnp.where(mine, q_t[...], 0.0), axis=1, keepdims=True), now.shape
+    )
+
+    def block(k_ref, d_ref, v_ref, offset):
+        s = k_ref[0].astype(F32) * q * jnp.exp(now - d_ref[0])
+        s = jnp.sum(s.reshape(heads, KEY_WIDTH, LANES), axis=1)
+        s = jnp.where(lane + offset < length - 1, s, 0.0).astype(BF16)
+        return lax.dot_general(s, v_ref[0], NT, preferred_element_type=F32)
+
+    hist[...] = block(k1, d1, v1, 0)
+
+    @pl.when(two)
+    def _():
+        hist[...] += block(k2, d2, v2, LANES)
+
+    weight = (q * jnp.exp(now))[:, :DV]
+    carried = jnp.sum((weight * st[0].reshape(keys, DV)).reshape(heads, KEY_WIDTH, DV), axis=1)
+    carried = jnp.concatenate([carried] * heads, axis=1)
+    qk = jnp.sum(jnp.where(mine, qk_t[...], 0.0), axis=1, keepdims=True)
+    whole = hist[...] + carried + qk * vn[pl.ds(step, 1), :]
+    own = lax.broadcasted_iota(jnp.int32, (heads, vals), 1) // DV
+    own = own == lax.broadcasted_iota(jnp.int32, (heads, vals), 0)
+    whole = jnp.where(own, whole, 0.0)
+    mean = jnp.sum(whole * whole, axis=1, keepdims=True) / DV
+    whole = whole * lax.rsqrt(mean + NORM_EPS)
+    raw[pl.ds(step, 1), :] = jnp.sum(whole, axis=0, keepdims=True)
+
+    @pl.when(step == rows - 1)
+    def _():
+        out_ref[...] = (raw[...] * gs[...]).astype(BF16)
+
+
+def attend(span_lengths, sums, square, bias, head_gain, keys, values, decays, state):
+    rows, heads = state.shape[:2]
+    kw, vw = heads * KEY_WIDTH, heads * DV
+    order = jnp.arange(rows, dtype=jnp.int32)
+    needed = jnp.where(span_lengths - 1 > LANES, order, 0)
+    last = jnp.max(jnp.where(order[None, :] <= order[:, None], needed[None, :], 0), axis=1)
+
+    def first(width):
+        return pl.BlockSpec((1, width, LANES), lambda i, ln, la: (i, 0, 0))
+
+    def second(width):
+        return pl.BlockSpec((1, width, LANES), lambda i, ln, la: (la[i], 0, 1))
+
+    def fixed(shape):
+        return pl.BlockSpec(shape, lambda i, ln, la: (0,) * len(shape))
+
+    return pl.pallas_call(
+        attend_kernel,
+        out_shape=jax.ShapeDtypeStruct((rows, vw), BF16),
+        grid_spec=pltpu.PrefetchScalarGridSpec(
+            num_scalar_prefetch=2,
+            grid=(rows,),
+            in_specs=[
+                fixed(sums.shape),
+                fixed(square.shape),
+                fixed((1, kw)),
+                fixed((1, DV)),
+                first(kw),
+                second(kw),
+                first(kw),
+                second(kw),
+                first(vw),
+                second(vw),
+                pl.BlockSpec((1, heads, KEY_WIDTH, DV), lambda i, ln, la: (i, 0, 0, 0)),
+            ],
+            out_specs=fixed((rows, vw)),
+            scratch_shapes=[
+                pltpu.VMEM((kw, LANES), F32),
+                pltpu.VMEM((kw, LANES), F32),
+                pltpu.VMEM((heads, LANES), F32),
+                pltpu.VMEM((rows, vw), F32),
+                pltpu.VMEM((rows, vw), F32),
+                pltpu.VMEM((kw, LANES), F32),
+                pltpu.VMEM((heads, vw), F32),
+                pltpu.VMEM((rows, vw), F32),
+            ],
+        ),
+        compiler_params=pltpu.CompilerParams(
+            dimension_semantics=("arbitrary",), vmem_limit_bytes=40 << 20
+        ),
+        name="attend",
+    )(
+        span_lengths, last, sums, square, bias.reshape(1, -1), head_gain.reshape(1, -1),
+        keys, keys, decays, decays, values, values, state,
+    )
+
+
+def finish_kernel(
+    mixed_ref, tok_ref, gain_ref, ow_ref, uw_ref, dw_ref, out_ref,
+    ow, uw, dw, gath, part, t_out, t_in, resid, scaled, sq_out, sq_in,
+    u_part, u_own, u_out, u_in, hid, total, t_out2, t_in2, done,
+    wsem, g_s, g_r, a_s, a_r, b_s, b_r, q_s, q_r, u_s, u_r, h_s, h_r, c_s, c_r, e_s, e_r,
+):
+    n, m = lax.axis_size("kv"), lax.axis_size("tp")
+    me, col = lax.axis_index("kv"), lax.axis_index("tp")
+    chunks = u_s.shape[1]
+    width = u_out.shape[2] // chunks
+    loads = [
+        pltpu.make_async_copy(ow_ref, ow, wsem.at[0]),
+    ]
+    for c in range(chunks):
+        at = pl.ds(c * width, width)
+        loads.append(pltpu.make_async_copy(uw_ref.at[:, at], uw.at[:, at], wsem.at[1 + c]))
+    loads.append(pltpu.make_async_copy(dw_ref, dw, wsem.at[1 + chunks]))
+    for load in loads:
+        load.start()
+    greet(("kv", "tp"))
+    copies = []
+
+    def wait_all(group):
+        for copy in group:
+            copy.wait_recv()
+        copies.extend(group)
+
+    group = [
+        send("kv", k, lambda p: mixed_ref, gath.at[me], g_s.at[k - 1], g_r.at[k - 1])
+        for k in SEND_ORDER(n)
+    ]
+    gath[me] = mixed_ref[...]
+    wait_all(group)
+    loads[0].wait()
+    rows = gath.shape[0] * gath.shape[1]
+
+    def over_tp(value, outgoing, incoming, ss, rs):
+        part[...] = value.reshape(part.shape)
+        outgoing[...] = value.reshape(part.shape).astype(BF16)
+        group = [
+            send("tp", k, lambda p: outgoing.at[p], incoming.at[k - 1], ss.at[k - 1], rs.at[k - 1])
+            for k in range(1, m)
+        ]
+        wait_all(group)
+        result = part[col]
+        for k in range(m - 1):
+            result = result + incoming[k].astype(F32)
+        return result
+
+    def to_tp(buffer, ss, rs):
+        group = [
+            send("tp", k, lambda p: buffer.at[col], buffer.at[col], ss.at[k - 1], rs.at[k - 1])
+            for k in range(1, m)
+        ]
+        wait_all(group)
+
+    x = gath[...].reshape(rows, gath.shape[2])
+    attn = over_tp(jnp.dot(x, ow[...], preferred_element_type=F32), t_out, t_in, a_s, a_r)
+    resid[col] = (tok_ref[col].astype(F32) + attn).astype(BF16)
+    to_tp(resid, b_s, b_r)
+    whole = resid[...].reshape(rows, resid.shape[2]).astype(F32)
+    square = jnp.sum(whole * whole, axis=1, keepdims=True)
+    sq_out[...] = jnp.broadcast_to(square, (rows, LANES)).reshape(sq_out.shape)
+    sq_group = [
+        send("kv", k, lambda p: sq_out.at[p], sq_in.at[k - 1], q_s.at[k - 1], q_r.at[k - 1])
+        for k in SEND_ORDER(n)
+    ]
+    scaled[...] = (whole * gain_ref[...]).astype(BF16)
+    groups = []
+    for c in range(chunks):
+        at = pl.ds(c * width, width)
+        loads[1 + c].wait()
+        got = jnp.dot(scaled[...], uw[:, at], preferred_element_type=F32)
+        got = got.reshape(u_part.shape)
+        u_part[...] = got
+        u_out[:, :, at] = got.astype(BF16)
+        groups.append(
+            [
+                send(
+                    "kv", k, lambda p: u_out.at[p, :, at], u_in.at[k - 1, :, at],
+                    u_s.at[k - 1, c], u_r.at[k - 1, c],
+                )
+                for k in SEND_ORDER(n)
+            ]
+        )
+        u_own[:, at] = u_part[me]
+    wait_all(sq_group)
+    square = sq_out[me]
+    for k in range(n - 1):
+        square = square + sq_in[k]
+    scale = lax.rsqrt(square[:, :1] / D + NORM_EPS)
+    hidden_groups = []
+    for c in range(chunks):
+        at = pl.ds(c * width, width)
+        wait_all(groups[c])
+        got = u_own[:, at]
+        for k in range(n - 1):
+            got = got + u_in[k, :, at].astype(F32)
+        hid[me, :, at] = jnp.square(jnp.maximum(got * scale, 0.0)).astype(BF16)
+        hidden_groups.append(
+            [
+                send(
+                    "kv", k, lambda p: hid.at[me, :, at], hid.at[me, :, at],
+                    h_s.at[k - 1, c], h_r.at[k - 1, c],
+                )
+                for k in SEND_ORDER(n)
+            ]
+        )
+    loads[1 + chunks].wait()
+    for c in range(chunks):
+        at = pl.ds(c * width, width)
+        wait_all(hidden_groups[c])
+        got = jnp.dot(
+            hid[:, :, at].reshape(rows, width), dw[at, :], preferred_element_type=F32
+        )
+        if c == 0:
+            total[...] = got
+        else:
+            total[...] += got
+    mixer = over_tp(total[...], t_out2, t_in2, c_s, c_r)
+    done[col] = (resid[col].astype(F32) + mixer).astype(BF16)
+    to_tp(done, e_s, e_r)
+    out_ref[...] = done[...]
+    for copy in copies:
+        copy.wait_send()
+
+
+def finish(mixed, tokens, gain, out_weight, up_weight, down_weight):
+    n, m = lax.axis_size("kv"), lax.axis_size("tp")
+    rows, feats = tokens.shape
+    vals, hidden = out_weight.shape[0], up_weight.shape[1]
+    own, share = rows // n, rows // m
+    chunks = 4
+    vmem = pl.BlockSpec(memory_space=pltpu.VMEM)
+    hbm = pl.BlockSpec(memory_space=pltpu.HBM)
+    dma = pltpu.SemaphoreType.DMA
+    out = pl.pallas_call(
+        finish_kernel,
+        out_shape=jax.ShapeDtypeStruct((m, share, feats), BF16),
+        in_specs=[vmem, vmem, vmem, hbm, hbm, hbm],
+        out_specs=vmem,
+        scratch_shapes=[
+            pltpu.VMEM(out_weight.shape, BF16),
+            pltpu.VMEM(up_weight.shape, BF16),
+            pltpu.VMEM(down_weight.shape, BF16),
+            pltpu.VMEM((n, own, vals), BF16),
+            pltpu.VMEM((m, share, feats), F32),
+            pltpu.VMEM((m, share, feats), BF16),
+            pltpu.VMEM((m - 1, share, feats), BF16),
+            pltpu.VMEM((m, share, feats), BF16),
+            pltpu.VMEM((rows, feats), BF16),
+            pltpu.VMEM((n, own, LANES), F32),
+            pltpu.VMEM((n - 1, own, LANES), F32),
+            pltpu.VMEM((n, own, hidden // chunks), F32),
+            pltpu.VMEM((own, hidden), F32),
+            pltpu.VMEM((n, own, hidden), BF16),
+            pltpu.VMEM((n - 1, own, hidden), BF16),
+            pltpu.VMEM((n, own, hidden), BF16),
+            pltpu.VMEM((rows, feats), F32),
+            pltpu.VMEM((m, share, feats), BF16),
+            pltpu.VMEM((m - 1, share, feats), BF16),
+            pltpu.VMEM((m, share, feats), BF16),
+            dma((2 + chunks,)),
+            dma((n - 1,)),
+            dma((n - 1,)),
+            dma((m - 1,)),
+            dma((m - 1,)),
+            dma((m - 1,)),
+            dma((m - 1,)),
+            dma((n - 1,)),
+            dma((n - 1,)),
+            dma((n - 1, chunks)),
+            dma((n - 1, chunks)),
+            dma((n - 1, chunks)),
+            dma((n - 1, chunks)),
+            dma((m - 1,)),
+            dma((m - 1,)),
+            dma((m - 1,)),
+            dma((m - 1,)),
+        ],
+        compiler_params=pltpu.CompilerParams(
+            collective_id=1, has_side_effects=True, vmem_limit_bytes=48 << 20
+        ),
+        name="finish",
+    )(
+        mixed, tokens.reshape(m, share, feats), gain.reshape(1, -1),
+        out_weight, up_weight, down_weight,
+    )
+    return out.reshape(rows, feats)
+
+
+def kernel_shards(
+    tokens,
+    span_lengths,
+    block_state,
+    key_cache,
+    value_cache,
+    decay_cache,
+    attn_gain,
+    query_weight,
+    key_weight,
+    value_weight,
+    gate_weight,
+    decay_matrix,
+    decay_offset_bias,
+    head_gain,
+    out_weight,
+    mixer_gain,
+    up_weight,
+    down_weight,
+):
+    weights = (query_weight, key_weight, value_weight, gate_weight, decay_matrix)
+    sums, square = project(tokens, attn_gain, weights)
+    mixed = attend(
+        span_lengths, sums, square, decay_offset_bias, head_gain,
+        key_cache, value_cache, decay_cache, block_state,
+    )
+    return finish(mixed, tokens, mixer_gain, out_weight, up_weight, down_weight)
+
+
+def fits(tokens, block_state, key_cache):
+    rows, heads = block_state.shape[:2]
+    share = tokens.shape[0] // lax.axis_size("tp")
+    return (
+        rows % 16 == 0
+        and share % 16 == 0
+        and heads % 8 == 0
+        and rows < LANES
+        and key_cache.shape[2] == 2 * LANES
+    )
 
 
 def shards(
@@ -32,6 +543,12 @@
     up_weight,
     down_weight,
 ):
+    if fits(tokens, block_state, key_cache):
+        return kernel_shards(
+            tokens, span_lengths, block_state, key_cache, value_cache, decay_cache,
+            attn_gain, query_weight, key_weight, value_weight, gate_weight, decay_matrix,
+            decay_offset_bias, head_gain, out_weight, mixer_gain, up_weight, down_weight,
+        )
     seq_count = block_state.shape[0]
     head_count = block_state.shape[1]
     span_size = key_cache.shape[2]

time: 294 us -> 156 us (0.53)
  waiting for transfers between devices: 172 us -> 0 us
  Pallas kernels: 0 us -> 139 us
  matrix products: 44.8 us -> 0 us
  blocking collectives: 32.2 us -> 0 us
  other arithmetic: 26.6 us -> 0.77 us
  between operations: 14 us -> 0.08 us
  local copies, waits for them, and re-layouts: 1.19 us -> 14.6 us
    pallas_call x0 -> x3, Pallas kernels: none -> 139 us  [the longest x1 77.2 us: finish(): pl.pallas_call(finish_kernel, out_shape=jax.ShapeDtypeStruct((m, share, f...]
    reduce_scatter x6 -> x0, waiting for transfers between devices: 77.9 us -> none  [the longest x1 33.3 us: shards(): lax.psum_scatter(up_part, 'kv', scatter_dimension=0, tiled=True)]
    psum x2 -> x0, waiting for transfers between devices: 66.9 us -> none  [the longest x1 34.7 us: shards(): attn_out = lax.psum(attn_terms, 'tp')]
    dot_general x10 -> x0, matrix products: 44.8 us -> none  [the longest x1 10.2 us: shards(): jnp.einsum('nhs,nhvs->nhv', scores_low, values_span, preferred_element_ty...]
    all_gather x1 -> x0, waiting for transfers between devices: 27.2 us -> none  [shards(): lax.all_gather(hidden_share, 'kv', axis=0, tiled=True)]
    reduce_sum x5 -> x0, other arithmetic: 19.3 us -> none  [the longest x1 9.67 us: shards(): jnp.sum(query[..., None] * keys_span.astype(jnp.float32) * factor, axis=2)]
    unnamed x21 -> x29, local copies, waits for them, and re-layouts: 0.63 us -> 14.6 us
    psum x1 -> x0, blocking collectives: 11.1 us -> none  [shards(): square_total = lax.psum(square_sum, 'kv')]
  transfers between devices with their start and end apart: 9 -> 0, of which waited for: 7 -> 0; matrix products, arithmetic and copies ran while one was open for 18% -> 0% of each run, Pallas kernels for 0% -> 0%
where the time goes in v1:
time: 156 us; the launch traced here: 155 us
  Pallas kernels  139 us (89%)
  local copies, waits for them, and re-layouts  14.6 us (9%)
    pallas_call x1, Pallas kernels, finish(): pl.pallas_call(finish_kernel, out_shape=jax.ShapeDtypeStruct((m, share, f...  77.2 us
    pallas_call x1, Pallas kernels, attend(): pl.pallas_call(attend_kernel, out_shape=jax.ShapeDtypeStruct((rows, vw),...  34.7 us
    pallas_call x1, Pallas kernels, project(): pl.pallas_call(functools.partial(project_kernel, parts), out_shape=(jax.S...  27.3 us
    unnamed x29, local copies, waits for them, and re-layouts  14.6 us

profile of v1, /device:TPU:1, one launch (start us, length us, event | category | flops | bytes accessed | tf_op | source)
XLA Modules:
  0.0 154.7 jit_solution(13062043754957074231)
XLA Ops:
  0.0 0.7 compare_select_fusion
  0.7 0.1 select_reduce_fusion.last_ref
  0.8 0.0 copy-start.1
  0.8 1.6 %copy-done.1 = bf16[1024,1024]{1,0:T(8,128)(2,1)S(1)} copy-done((bf16[1024,1024]{1,0:T(8,128)(2,1)S(1)}, bf16[1024,1024]{1,0:T(8,128)(2,1)}, u32[]{:S(2)}) %copy-start.1) | copy-done | bytes 2097176
  2.4 0.0 copy-start.2
  2.4 1.6 %copy-done.2 = bf16[1024,1024]{1,0:T(8,128)(2,1)S(1)} copy-done((bf16[1024,1024]{1,0:T(8,128)(2,1)S(1)}, bf16[1024,1024]{1,0:T(8,128)(2,1)}, u32[]{:S(2)}) %copy-start.2) | copy-done | bytes 2097176
  4.0 0.0 copy-start.4
  4.0 0.9 copy-done.4
  4.9 0.0 copy-start.6
  4.9 1.2 copy-done.6
  6.1 0.0 copy-start.7
  6.1 1.2 copy-done.7
  7.4 0.0 copy-start.8
  7.4 1.2 copy-done.8
  8.6 0.0 copy-start.9
  8.6 0.7 copy-done.9
  9.3 27.3 %project.1 = (f32[32,3584]{1,0:T(8,128)S(1)}, f32[32,128]{1,0:T(8,128)S(1)}) custom-call(bf16[128,1024]{1,0:T(8,128)(2,1)S(1)} %copy-done.4, f32[1,1024]{1,0:T(1,128)S(1)} %bitcast.8, bf16[1024,512]{1,0:T(8,128)(2,1)S(1)} %copy-done.6, bf16[1024,512]{1,0:T(8,128)(2,1)S(1)} %copy-done.7, bf16[1024,1024]{1,0:T(8,128)(2,1)S(1)} %copy-done.1, ...), custom_call_target="tpu_custom_call" | custom-call | tf_op jit(solution)/shard_map/project/pallas_call | solution.py:121
  36.6 0.0 copy-start
  36.6 3.4 %copy-done = bf16[32,512,256]{2,1,0:T(8,128)(2,1)S(1)} copy-done((bf16[32,512,256]{2,1,0:T(8,128)(2,1)S(1)}, bf16[32,512,256]{2,1,0:T(8,128)(2,1)}, u32[]{:S(2)}) %copy-start) | copy-done | bytes 8388632
  40.0 0.0 copy-start.11
  40.0 0.7 copy-done.11
  40.6 0.0 copy-start.12
  40.7 0.7 copy-done.12
  41.3 0.0 copy-start.13
  41.3 0.7 copy-done.13
  42.0 0.0 copy-start.3
  42.0 0.0 copy-start.5
  42.0 0.0 copy-start.10
  42.0 34.7 %attend.1.mixed_ref = bf16[32,1024]{1,0:T(8,128)(2,1)S(1)} custom-call(s32[32]{0:T(128)S(1)} %copy-done.12, s32[32]{0:T(128)S(1)} %select_reduce_fusion.last_ref, f32[32,3584]{1,0:T(8,128)S(1)} %get-tuple-element.7.sum_ref, f32[32,128]{1,0:T(8,128)S(1)} %get-tuple-element.8.sq_ref, f32[1,512]{1,0:T(1,128)S(1)} %bitcast.10, f32[1,64]{1,0:T(1,128)S(1)} %bitcast.11, ...), custom_call_target="tpu_custom_call" | custom-call | tf_op jit(solution)/shard_map/attend/pallas_call | solution.py:253
  76.7 0.0 copy-done.3
  76.7 0.0 copy-done.5
  76.7 0.0 copy-done.10
  76.7 77.2 %finish.1 = bf16[4,32,1024]{2,1,0:T(8,128)(2,1)S(1)} custom-call(bf16[32,1024]{1,0:T(8,128)(2,1)S(1)} %attend.1.mixed_ref, bf16[4,32,1024]{2,1,0:T(8,128)(2,1)S(1)} %bitcast.6, f32[1,1024]{1,0:T(1,128)S(1)} %bitcast.9, bf16[1024,1024]{1,0:T(8,128)(2,1)S(1)} %copy-done.3, bf16[1024,4096]{1,0:T(8,128)(2,1)} %uw_ref.1, bf16[4096,1024]{1,0:T(8,128)(2,1)} %dw_ref.1), custom_call_target="tpu_custom_call" | custom-call | tf_op jit(solution)/shard_map/finish/pallas_call | solution.py:430
  154.0 0.7 copy.20
Async XLA Ops:
  0.8 1.6 %copy-start.1 = (bf16[1024,1024]{1,0:T(8,128)(2,1)S(1)}, bf16[1024,1024]{1,0:T(8,128)(2,1)}, u32[]{:S(2)}) copy-start(bf16[1024,1024]{1,0:T(8,128)(2,1)} %refs_2_.1) | copy-start | bytes 6291460
  2.4 1.6 %copy-start.2 = (bf16[1024,1024]{1,0:T(8,128)(2,1)S(1)}, bf16[1024,1024]{1,0:T(8,128)(2,1)}, u32[]{:S(2)}) copy-start(bf16[1024,1024]{1,0:T(8,128)(2,1)} %refs_3_.1) | copy-start | bytes 6291460
  4.0 0.9 copy-start.4
  4.9 1.2 copy-start.6
  6.1 1.2 copy-start.7
  7.4 1.2 copy-start.8
  8.6 0.7 copy-start.9
  36.6 3.4 %copy-start = (bf16[32,512,256]{2,1,0:T(8,128)(2,1)S(1)}, bf16[32,512,256]{2,1,0:T(8,128)(2,1)}, u32[]{:S(2)}) copy-start(bf16[32,512,256]{2,1,0:T(8,128)(2,1)} %k2.1) | copy-start | bytes 25165828
  40.0 0.7 copy-start.11
  40.6 0.7 copy-start.12
  41.3 0.7 copy-start.13
  42.0 34.7 %copy-start.3 = (bf16[1024,1024]{1,0:T(8,128)(2,1)S(1)}, bf16[1024,1024]{1,0:T(8,128)(2,1)}, u32[]{:S(2)}) copy-start(bf16[1024,1024]{1,0:T(8,128)(2,1)} %ow_ref.1) | copy-start | bytes 6291460
  42.0 34.7 %copy-start.5 = (bf16[128,1024]{1,0:T(8,128)(2,1)S(1)}, bf16[128,1024]{1,0:T(8,128)(2,1)}, u32[]{:S(2)}) copy-start(bf16[128,1024]{1,0:T(8,128)(2,1)} %tok_ref.1) | copy-start | bytes 786436
  42.0 34.7 %copy-start.10 = (f32[1024]{0:T(1024)S(1)}, f32[1024]{0:T(1024)}, u32[]{:S(2)}) copy-start(f32[1024]{0:T(1024)} %param.33) | copy-start | bytes 12292

commit v2 on v1

--- a/solution.py
+++ b/solution.py
@@ -140,7 +140,7 @@
             pltpu.SemaphoreType.DMA((n - 1,)),
         ],
         compiler_params=pltpu.CompilerParams(
-            collective_id=0, has_side_effects=True, vmem_limit_bytes=40 << 20
+            collective_id=0, has_side_effects=True, vmem_limit_bytes=62 << 20
         ),
         name="project",
     )(tokens, gain.reshape(1, -1), *weights)
@@ -150,8 +150,8 @@
 
 
 def attend_kernel(
-    len_ref, last_ref, sum_ref, sq_ref, bias_ref, hg_ref, k1, k2, d1, d2, v1, v2, st,
-    out_ref, q_t, ld_t, qk_t, vn, gs, now_s, hist, raw,
+    len_ref, last_ref, sum_ref, sq_ref, bias_ref, hg_ref, k1, k2a, k2b, d1, d2a, d2b,
+    v1, v2a, v2b, st, out_ref, q_t, ld_t, qk_t, vn, gs, now_s, q_s, hist, raw,
 ):
     step = pl.program_id(0)
     rows = out_ref.shape[0]
@@ -183,53 +183,49 @@
             preferred_element_type=F32,
         )
 
-    length = len_ref[step]
-    two = length - 1 > LANES
-    mine = lane == step
-    own_decay = jnp.where(mine, ld_t[...], 0.0)
-
-    @pl.when(two)
-    def _():
-        prev = jnp.where(lane + LANES == length - 2, d2[0], 0.0)
-        col = jnp.sum(own_decay + prev, axis=1, keepdims=True)
-        now_s[...] = jnp.broadcast_to(col, now_s.shape)
-
-    @pl.when(jnp.logical_not(two))
-    def _():
-        prev = jnp.where(lane == length - 2, d1[0], 0.0)
-        col = jnp.sum(own_decay + prev, axis=1, keepdims=True)
-        now_s[...] = jnp.broadcast_to(col, now_s.shape)
-
-    now = now_s[...]
-    q = jnp.broadcast_to(
-        jnp.sum(jnp.where(mine, q_t[...], 0.0), axis=1, keepdims=True), now.shape
-    )
-
-    def block(k_ref, d_ref, v_ref, offset):
-        s = k_ref[0].astype(F32) * q * jnp.exp(now - d_ref[0])
+    seconds = ((k2a, d2a, v2a), (k2b, d2b, v2b))
+    lengths = [len_ref[2 * step + j] for j in range(2)]
+    mine = [lane == 2 * step + j for j in range(2)]
+    wide = (keys, LANES)
+
+    def block(j, k, d, v, offset):
+        s = k.astype(F32) * q_s[j] * jnp.exp(now_s[j] - d)
         s = jnp.sum(s.reshape(heads, KEY_WIDTH, LANES), axis=1)
-        s = jnp.where(lane + offset < length - 1, s, 0.0).astype(BF16)
-        return lax.dot_general(s, v_ref[0], NT, preferred_element_type=F32)
-
-    hist[...] = block(k1, d1, v1, 0)
-
-    @pl.when(two)
-    def _():
-        hist[...] += block(k2, d2, v2, LANES)
-
-    weight = (q * jnp.exp(now))[:, :DV]
-    carried = jnp.sum((weight * st[0].reshape(keys, DV)).reshape(heads, KEY_WIDTH, DV), axis=1)
-    carried = jnp.concatenate([carried] * heads, axis=1)
-    qk = jnp.sum(jnp.where(mine, qk_t[...], 0.0), axis=1, keepdims=True)
-    whole = hist[...] + carried + qk * vn[pl.ds(step, 1), :]
+        s = jnp.where(lane + offset < lengths[j] - 1, s, 0.0).astype(BF16)
+        return lax.dot_general(s, v, NT, preferred_element_type=F32)
+
+    for j in range(2):
+        prev = jnp.where(lane == lengths[j] - 2, d1[j], 0.0)
+        prev = prev + jnp.where(lane + LANES == lengths[j] - 2, seconds[j][1][0], 0.0)
+        own_decay = jnp.where(mine[j], ld_t[...], 0.0)
+        now_s[j] = jnp.broadcast_to(jnp.sum(prev + own_decay, axis=1, keepdims=True), wide)
+        q = jnp.sum(jnp.where(mine[j], q_t[...], 0.0), axis=1, keepdims=True)
+        q_s[j] = jnp.broadcast_to(q, wide)
+    for j in range(2):
+        hist[j] = block(j, k1[j], d1[j], v1[j], 0)
+    for j in range(2):
+
+        @pl.when(lengths[j] - 1 > LANES)
+        def _(j=j):
+            k2, d2, v2 = seconds[j]
+            hist[j] += block(j, k2[0], d2[0], v2[0], LANES)
+
     own = lax.broadcasted_iota(jnp.int32, (heads, vals), 1) // DV
     own = own == lax.broadcasted_iota(jnp.int32, (heads, vals), 0)
-    whole = jnp.where(own, whole, 0.0)
-    mean = jnp.sum(whole * whole, axis=1, keepdims=True) / DV
-    whole = whole * lax.rsqrt(mean + NORM_EPS)
-    raw[pl.ds(step, 1), :] = jnp.sum(whole, axis=0, keepdims=True)
-
-    @pl.when(step == rows - 1)
+    for j in range(2):
+        weight = (q_s[j] * jnp.exp(now_s[j]))[:, :DV]
+        carried = weight * st[j].reshape(keys, DV)
+        carried = jnp.sum(carried.reshape(heads, KEY_WIDTH, DV), axis=1)
+        carried = jnp.concatenate([carried] * heads, axis=1)
+        qk = jnp.sum(jnp.where(mine[j], qk_t[...], 0.0), axis=1, keepdims=True)
+        row = pl.ds(2 * step + j, 1)
+        whole = hist[j] + carried + qk * vn[row, :]
+        whole = jnp.where(own, whole, 0.0)
+        mean = jnp.sum(whole * whole, axis=1, keepdims=True) / DV
+        whole = whole * lax.rsqrt(mean + NORM_EPS)
+        raw[row, :] = jnp.sum(whole, axis=0, keepdims=True)
+
+    @pl.when(step == pl.num_programs(0) - 1)
     def _():
         out_ref[...] = (raw[...] * gs[...]).astype(BF16)
 
@@ -238,14 +234,15 @@
     rows, heads = state.shape[:2]
     kw, vw = heads * KEY_WIDTH, heads * DV
     order = jnp.arange(rows, dtype=jnp.int32)
-    needed = jnp.where(span_lengths - 1 > LANES, order, 0)
-    last = jnp.max(jnp.where(order[None, :] <= order[:, None], needed[None, :], 0), axis=1)
+    needed = jnp.where(span_lengths - 1 > LANES, order, order % 2)
+    before = (order[None, :] <= order[:, None]) & (order[None, :] % 2 == order[:, None] % 2)
+    last = jnp.max(jnp.where(before, needed[None, :], 0), axis=1)
 
     def first(width):
-        return pl.BlockSpec((1, width, LANES), lambda i, ln, la: (i, 0, 0))
-
-    def second(width):
-        return pl.BlockSpec((1, width, LANES), lambda i, ln, la: (la[i], 0, 1))
+        return pl.BlockSpec((2, width, LANES), lambda i, ln, la: (i, 0, 0))
+
+    def second(width, j):
+        return pl.BlockSpec((1, width, LANES), lambda i, ln, la: (la[2 * i + j], 0, 1))
 
     def fixed(shape):
         return pl.BlockSpec(shape, lambda i, ln, la: (0,) * len(shape))
@@ -255,19 +252,22 @@
         out_shape=jax.ShapeDtypeStruct((rows, vw), BF16),
         grid_spec=pltpu.PrefetchScalarGridSpec(
             num_scalar_prefetch=2,
-            grid=(rows,),
+            grid=(rows // 2,),
             in_specs=[
                 fixed(sums.shape),
                 fixed(square.shape),
                 fixed((1, kw)),
                 fixed((1, DV)),
                 first(kw),
-                second(kw),
+                second(kw, 0),
+                second(kw, 1),
                 first(kw),
-                second(kw),
+                second(kw, 0),
+                second(kw, 1),
                 first(vw),
-                second(vw),
-                pl.BlockSpec((1, heads, KEY_WIDTH, DV), lambda i, ln, la: (i, 0, 0, 0)),
+                second(vw, 0),
+                second(vw, 1),
+                pl.BlockSpec((2, heads, KEY_WIDTH, DV), lambda i, ln, la: (i, 0, 0, 0)),
             ],
             out_specs=fixed((rows, vw)),
             scratch_shapes=[
@@ -276,18 +276,19 @@
                 pltpu.VMEM((heads, LANES), F32),
                 pltpu.VMEM((rows, vw), F32),
                 pltpu.VMEM((rows, vw), F32),
-                pltpu.VMEM((kw, LANES), F32),
-                pltpu.VMEM((heads, vw), F32),
+                pltpu.VMEM((2, kw, LANES), F32),
+                pltpu.VMEM((2, kw, LANES), F32),
+                pltpu.VMEM((2, heads, vw), F32),
                 pltpu.VMEM((rows, vw), F32),
             ],
         ),
         compiler_params=pltpu.CompilerParams(
-            dimension_semantics=("arbitrary",), vmem_limit_bytes=40 << 20
+            dimension_semantics=("arbitrary",), vmem_limit_bytes=62 << 20
         ),
         name="attend",
     )(
         span_lengths, last, sums, square, bias.reshape(1, -1), head_gain.reshape(1, -1),
-        keys, keys, decays, decays, values, values, state,
+        keys, keys, keys, decays, decays, decays, values, values, values, state,
     )
 
 
@@ -359,6 +360,16 @@
         for k in SEND_ORDER(n)
     ]
     scaled[...] = (whole * gain_ref[...]).astype(BF16)
+
+    def toward(bit, ref, ss, rs):
+        peer = me + bit - 2 * bit * (me // bit % 2)
+        copy = pltpu.make_async_remote_copy(
+            src_ref=ref(peer), dst_ref=ref(peer), send_sem=ss, recv_sem=rs,
+            device_id={"kv": peer}, device_id_type=MESH,
+        )
+        copy.start()
+        return copy
+
     groups = []
     for c in range(chunks):
         at = pl.ds(c * width, width)
@@ -392,17 +403,21 @@
         hid[me, :, at] = jnp.square(jnp.maximum(got * scale, 0.0)).astype(BF16)
         hidden_groups.append(
             [
-                send(
-                    "kv", k, lambda p: hid.at[me, :, at], hid.at[me, :, at],
-                    h_s.at[k - 1, c], h_r.at[k - 1, c],
-                )
-                for k in SEND_ORDER(n)
+                toward(2, lambda p: hid.at[me, :, at], h_s.at[0, c], h_r.at[0, c]),
+                toward(1, lambda p: hid.at[me, :, at], h_s.at[1, c], h_r.at[1, c]),
             ]
+        )
+    for c in range(chunks):
+        at = pl.ds(c * width, width)
+        wait_all(hidden_groups[c][:1])
+        far = me + 2 - 4 * (me // 2)
+        hidden_groups[c].append(
+            toward(1, lambda p: hid.at[far, :, at], h_s.at[2, c], h_r.at[2, c])
         )
     loads[1 + chunks].wait()
     for c in range(chunks):
         at = pl.ds(c * width, width)
-        wait_all(hidden_groups[c])
+        wait_all(hidden_groups[c][1:])
         got = jnp.dot(
             hid[:, :, at].reshape(rows, width), dw[at, :], preferred_element_type=F32
         )
@@ -472,7 +487,7 @@
             dma((m - 1,)),
         ],
         compiler_params=pltpu.CompilerParams(
-            collective_id=1, has_side_effects=True, vmem_limit_bytes=48 << 20
+            collective_id=1, has_side_effects=True, vmem_limit_bytes=62 << 20
         ),
         name="finish",
     )(
@@ -515,7 +530,8 @@
     rows, heads = block_state.shape[:2]
     share = tokens.shape[0] // lax.axis_size("tp")
     return (
-        rows % 16 == 0
+        lax.axis_size("kv") == 4
+        and rows % 16 == 0
         and share % 16 == 0
         and heads % 8 == 0
         and rows < LANES

time: 156 us -> 130 us (0.83)
  local copies, waits for them, and re-layouts: 14.6 us -> 1.67 us
  Pallas kernels: 139 us -> 127 us
    unnamed x29 -> x1, local copies, waits for them, and re-layouts: 14.6 us -> 1.67 us
    pallas_call x1, Pallas kernels: 34.7 us -> 26.5 us  [attend(): pl.pallas_call(attend_kernel, out_shape=jax.ShapeDtypeStruct((rows, vw),...]
    pallas_call x1, Pallas kernels: 77.2 us -> 73.1 us  [finish(): pl.pallas_call(finish_kernel, out_shape=jax.ShapeDtypeStruct((m, share, f...]
where the time goes in v2:
time: 130 us
  Pallas kernels  127 us (98%)
  local copies, waits for them, and re-layouts  1.67 us (1%)
  other arithmetic  1.43 us (1%)
    pallas_call x1, Pallas kernels, finish(): pl.pallas_call(finish_kernel, out_shape=jax.ShapeDtypeStruct((m, share, f...  73.1 us
    pallas_call x1, Pallas kernels, project(): pl.pallas_call(functools.partial(project_kernel, parts), out_shape=(jax.S...  27.5 us
    pallas_call x1, Pallas kernels, attend(): pl.pallas_call(attend_kernel, out_shape=jax.ShapeDtypeStruct((rows, vw),...  26.5 us

profile of v2, /device:TPU:1, one launch (start us, length us, event | category | flops | bytes accessed | tf_op | source)
XLA Modules:
  0.0 130.2 jit_solution(13409519112639355076)
XLA Ops:
  0.0 0.7 compare_select_fusion
  0.7 0.8 select_reduce_fusion.last_ref
  1.4 27.5 %project.1 = (f32[32,3584]{1,0:T(8,128)}, f32[32,128]{1,0:T(8,128)}) custom-call(bf16[128,1024]{1,0:T(8,128)(2,1)} %tok_ref.1, f32[1,1024]{1,0:T(1,128)} %bitcast.8, bf16[1024,512]{1,0:T(8,128)(2,1)} %refs_0_.1, bf16[1024,512]{1,0:T(8,128)(2,1)} %refs_1_.1, bf16[1024,1024]{1,0:T(8,128)(2,1)} %refs_2_.1, bf16[1024,1024]{1,0:T(8,128)(2,1)} %refs_3_.1, ...), custom_call_target="tpu_custom_call" | custom-call | tf_op jit(solution)/shard_map/project/pallas_call | solution.py:121
  29.0 26.5 %attend.1.mixed_ref = bf16[32,1024]{1,0:T(8,128)(2,1)} custom-call(s32[32]{0:T(128)} %len_ref.1, s32[32]{0:T(128)} %select_reduce_fusion.last_ref, f32[32,3584]{1,0:T(8,128)} %get-tuple-element.7.sum_ref, f32[32,128]{1,0:T(8,128)} %get-tuple-element.8.sq_ref, f32[1,512]{1,0:T(1,128)} %bitcast.10, f32[1,64]{1,0:T(1,128)} %bitcast.11, ...), custom_call_target="tpu_custom_call" | custom-call | tf_op jit(solution)/shard_map/attend/pallas_call | solution.py:250
  55.5 73.1 %finish.1 = bf16[4,32,1024]{2,1,0:T(8,128)(2,1)} custom-call(bf16[32,1024]{1,0:T(8,128)(2,1)} %attend.1.mixed_ref, bf16[4,32,1024]{2,1,0:T(8,128)(2,1)} %bitcast.6, f32[1,1024]{1,0:T(1,128)} %bitcast.9, bf16[1024,1024]{1,0:T(8,128)(2,1)} %ow_ref.1, bf16[1024,4096]{1,0:T(8,128)(2,1)} %uw_ref.1, bf16[4096,1024]{1,0:T(8,128)(2,1)} %dw_ref.1), custom_call_target="tpu_custom_call" | custom-call | tf_op jit(solution)/shard_map/finish/pallas_call | solution.py:445
  128.5 1.7 %copy.20 = bf16[128,1024]{1,0:T(8,128)(2,1)} copy(bf16[128,1024]{1,0:T(8,128)(2,1)} %bitcast.7) | data formatting | bytes 524288
